TPU v7x, 32 devices: a whole 2x2x4 slice. The times are simulated.
32 devices in a mesh: dp: 4 (over y, x), kv: 4 (over z), tp: 2 (over core).
Axes of the slice: x: 2, y: 2, z: 4, core: 2. Of those that a mesh axis runs over, the one named last changes fastest.
Arguments:
- tokens: bfloat16 [128, 4096], P('dp', ('kv', 'tp')), parts along dimension 0, may hold values from -12 to 12
- norm_gain: float32 [4096], replicated, may hold values from 0.1 to 1.9
- w_query: bfloat16 [4096, 3072], P(None, ('kv', 'tp')), may hold values from -0.09375 to 0.09375
- w_key: bfloat16 [4096, 3072], P(None, ('kv', 'tp')), may hold values from -0.09375 to 0.09375
- w_value: bfloat16 [4096, 3072], P(None, ('kv', 'tp')), may hold values from -0.09375 to 0.09375
- w_gate: bfloat16 [4096, 3072], P(None, ('kv', 'tp')), may hold values from -0.09375 to 0.09375
- w_output: bfloat16 [3072, 4096], P(None, ('kv', 'tp')), may hold values from -0.109375 to 0.109375
- decay_rate: float32 [24], replicated, may hold values from 0.003 to 2
- state: float32 [32, 24, 128, 128], P(('dp', 'kv', 'tp')), parts along dimension 0, may hold values from -0.54 to 0.54
- prev_keys: bfloat16 [32, 4, 3072], P(('dp', 'kv', 'tp')), parts along dimension 0, may hold values from -0.5390625 to 0.5390625
- prev_values: bfloat16 [32, 4, 3072], P(('dp', 'kv', 'tp')), parts along dimension 0, may hold values from -6 to 6
- accepted: int32 [32], P(('dp', 'kv', 'tp')), parts along dimension 0, may hold values from 0 to 4
- parents: int32 [32, 4], P(('dp', 'kv', 'tp')), parts along dimension 0, may hold values from -1 to 2, as said below
- seq_length: int32 [32], P(('dp', 'kv', 'tp')), parts along dimension 0, may hold values from 1 to 8191
Outputs:
- output: bfloat16 [128, 4096], P('dp', ('kv', 'tp')), parts along dimension 0
- carried: float32 [32, 24, 128, 128], P(('dp', 'kv', 'tp')), parts along dimension 0
There are 4 independent parts, one for each index of `dp`. A program takes and returns all parts, laid end to end along the dimension named above; an argument that names none is the same for every part. Nothing has to cross between parts.
Inputs may be any that keep to these rules, and one draw needn't show every extreme that they name: parents[s, i] is -1 or an earlier proposal of the same sequence; proposal 0 has -1.
All inputs are finite; a program needn't handle non-finite values.
Results may differ from a plain program's by a relative error of at most 0.013.
Values may be sent and summed in bfloat16 or wider, within the bound.
A program may use at most 64 MiB of HBM per device.

v0:
```python
import jax
import jax.numpy as jnp
from jax import lax
from jax.sharding import PartitionSpec as P

EPS = 1e-06
HIGH = lax.Precision.HIGHEST


def rotate(tensor, positions):
    half_dim = tensor.shape[-1] // 2
    frequency = 10000.0 ** (-jnp.arange(half_dim, dtype=jnp.float32) / half_dim)
    angles = positions[:, :, None] * frequency[None, None, :]
    cosine = jnp.cos(angles)[:, :, None, :]
    sine_part = jnp.sin(angles)[:, :, None, :]
    first = tensor[..., :half_dim]
    second = tensor[..., half_dim:]
    return jnp.concatenate(
        [first * cosine - second * sine_part, second * cosine + first * sine_part], axis=-1
    )


def ancestry_of(parents):
    props = parents.shape[1]
    linked = (parents[:, :, None] == jnp.arange(props, dtype=jnp.int32)[None, None, :]).astype(
        jnp.float32
    )
    identity = jnp.broadcast_to(jnp.eye(props, dtype=jnp.float32), linked.shape)
    ancestry = identity
    power = identity
    for hop in range(props - 1):
        power = jnp.einsum("bij,bjk->bik", power, linked, precision=HIGH)
        ancestry = ancestry + power
    depths = jnp.sum(ancestry, axis=-1) - 1.0
    return (ancestry, depths)


def advance(state, prev_keys, prev_values, accepted, decays):
    nseq, props, width = prev_keys.shape
    heads = decays.shape[0]
    head_dim = width // heads
    old_keys = prev_keys.astype(jnp.float32).reshape(nseq, props, heads, head_dim)
    old_values = prev_values.astype(jnp.float32).reshape(nseq, props, heads, head_dim)
    steps_done = accepted.astype(jnp.float32)[:, None]
    index = jnp.arange(props, dtype=jnp.float32)[None, :]
    age = jnp.maximum(steps_done - 1.0 - index, 0.0)
    weights = jnp.where(
        (index < steps_done)[:, :, None], jnp.exp(-decays[None, None, :] * age[:, :, None]), 0.0
    )
    kept = jnp.exp(-decays[None, :] * steps_done)
    added = jnp.einsum("bphd,bphe->bhde", old_keys * weights[..., None], old_values, precision=HIGH)
    return kept[:, :, None, None] * state + added


def retain(queries, key_rows, val_rows, gate_rows, decays, carried, parents, accepted, seq_length):
    nseq, props, heads, head_dim = queries.shape
    ancestry, depths = ancestry_of(parents)
    positions = (seq_length + accepted).astype(jnp.float32)[:, None] + depths
    rotated_q = rotate(queries.astype(jnp.float32), positions)
    rotated_k = rotate(key_rows.astype(jnp.float32), positions) * head_dim ** (-0.5)
    scores = jnp.einsum("bihd,bjhd->bhij", rotated_q, rotated_k, precision=HIGH)
    spacing = jnp.maximum(depths[:, :, None] - depths[:, None, :], 0.0)
    weighting = ancestry[:, None] * jnp.exp(-decays[None, :, None, None] * spacing[:, None])
    within = jnp.einsum(
        "bhij,bjhe->bihe", scores * weighting, val_rows.astype(jnp.float32), precision=HIGH
    )
    state_scale = jnp.exp(-decays[None, None, :] * (depths[:, :, None] + 1.0))
    from_state = (
        jnp.einsum("bihd,bhde->bihe", rotated_q, carried, precision=HIGH) * state_scale[..., None]
    )
    mixed_raw = within + from_state
    average = jnp.mean(mixed_raw, axis=-1, keepdims=True)
    centred = mixed_raw - average
    variance = jnp.mean(centred * centred, axis=-1, keepdims=True)
    normed = (centred * lax.rsqrt(variance + EPS)).reshape(nseq * props, heads * head_dim)
    gates = gate_rows.astype(jnp.float32).reshape(nseq * props, heads * head_dim)
    return (normed * jax.nn.silu(gates)).astype(jnp.bfloat16)


def per_device(
    tokens,
    norm_gain,
    w_query,
    w_key,
    w_value,
    w_gate,
    w_output,
    decay_rate,
    state,
    prev_keys,
    prev_values,
    accepted,
    parents,
    seq_length,
):
    weights = jnp.concatenate([w_query, w_key, w_value, w_gate], axis=1)
    columns = weights.shape[1]
    whole = lax.all_gather(tokens, ("kv", "tp"), axis=1, tiled=True).astype(jnp.float32)
    scale = lax.rsqrt(jnp.mean(whole * whole, axis=1, keepdims=True) + EPS)
    full_normed = (whole * scale * norm_gain[None, :]).astype(jnp.bfloat16)
    projected = jnp.dot(full_normed, weights, preferred_element_type=jnp.float32)
    rows_count = tokens.shape[0]
    projected = projected.astype(jnp.bfloat16).reshape(rows_count, 4, columns // 4)
    regrouped = lax.all_to_all(projected, ("kv", "tp"), split_axis=0, concat_axis=2, tiled=True)
    nseq = state.shape[0]
    heads = decay_rate.shape[0]
    head_dim = state.shape[2]
    props = parents.shape[1]

    def shaped(role):
        return regrouped[:, role].reshape(nseq, props, heads, head_dim)

    carried = advance(state, prev_keys, prev_values, accepted, decay_rate)
    mixed = retain(
        shaped(0),
        shaped(1),
        shaped(2),
        shaped(3),
        decay_rate,
        carried,
        parents,
        accepted,
        seq_length,
    )
    output = jnp.dot(
        lax.all_gather(mixed, ("kv", "tp"), axis=0, tiled=True),
        w_output,
        preferred_element_type=jnp.float32,
    ).astype(jnp.bfloat16)
    return (output, carried)


def solution(mesh):
    placed = (
        P("dp", ("kv", "tp")),
        P(),
        P(None, ("kv", "tp")),
        P(None, ("kv", "tp")),
        P(None, ("kv", "tp")),
        P(None, ("kv", "tp")),
        P(None, ("kv", "tp")),
        P(),
        P(("dp", "kv", "tp"), None, None, None),
        P(("dp", "kv", "tp"), None, None),
        P(("dp", "kv", "tp"), None, None),
        P(("dp", "kv", "tp")),
        P(("dp", "kv", "tp"), None),
        P(("dp", "kv", "tp")),
    )
    return jax.shard_map(
        per_device,
        mesh=mesh,
        in_specs=placed,
        out_specs=(P("dp", ("kv", "tp")), P(("dp", "kv", "tp"), None, None, None)),
        check_vma=False,
    )
```

profile of v0, /device:TPU:1, one launch (start us, length us, event | category | flops | bytes accessed | tf_op | source)
XLA Modules:
  0.0 55.6 jit_solution(4770530740804355256)
XLA Ops:
  0.6 0.0 copy-start
  0.6 16.1 %all_gather.6 = bf16[32,4096]{1,0:T(8,128)(2,1)S(1)} all-gather(bf16[32,512]{1,0:T(8,128)(2,1)} %param.14), channel_id=1, replica_groups=mesh['dp'=4,'kv'=4,'tp'=2] {'kv','tp'}, dimensions={1}, use_global_device_ids=true | all-gather | bytes 294912 | tf_op jit(solution)/shard_map/all_gather | solution.py:98
  16.8 0.2 fusion.20
  16.9 0.0 copy-start.4
  17.0 0.0 copy-start.1
  17.0 0.0 copy-start.2
  17.0 6.3 %fusion.8 = bf16[32,1536]{1,0:T(8,128)(2,1)S(1)} fusion(bf16[4096,384]{1,0:T(8,128)(2,1)} %param.19, bf16[4096,384]{1,0:T(8,128)(2,1)} %param.18, bf16[4096,384]{1,0:T(8,128)(2,1)} %param.17, bf16[4096,384]{1,0:T(8,128)(2,1)} %param.16, bf16[32,4096]{1,0:T(8,128)(2,1)S(1)} %all_gather.6, f32[4096]{0:T(1024)} %param.15, f32[32]{0:T(128)S(1)} %add_rsqrt_fusion.1), kind=kOutput, calls=%fused_computation.8 | convolution fusion | flops 453558272 | bytes 12959872 | tf_op jit(solution)/shard_map/dot_general | solution.py:101
  23.3 0.7 %reshape.477 = bf16[32,4,384]{2,1,0:T(4,128)(2,1)} reshape(bf16[32,1536]{1,0:T(8,128)(2,1)S(1)} %fusion.8) | data formatting | bytes 196608 | tf_op jit(solution)/shard_map/reshape | solution.py:103
  24.0 4.8 %all-to-all-start = ((bf16[32,4,384]{2,1,0:T(4,128)(2,1)}), bf16[32,4,384]{2,1,0:T(4,128)(2,1)S(1)}, u32[]{:S(2)}, u32[]{:S(2)}) async-start(bf16[32,4,384]{2,1,0:T(4,128)(2,1)} %reshape.477), calls=%async_computation | async-start | bytes 196608 | tf_op jit(solution)/shard_map/all_to_all | solution.py:104
  30.2 0.0 copy-done.3
  30.2 0.0 copy-done.4
  30.2 0.3 fusion.39
  30.5 0.3 fusion.38
  30.7 0.3 fusion.50
  31.0 0.1 copy.41
  31.1 0.1 multiply_cosine_fusion
  31.2 0.1 multiply_exponential_fusion
  31.3 0.0 copy-done.1
  31.3 0.0 copy-done.2
  31.3 4.2 %bitcast_add_fusion = f32[1,24,128,128]{3,2,1,0:T(8,128)} fusion(f32[1,24,128,128]{3,2,1,0:T(8,128)} %param.22, f32[24]{0:T(128)S(1)} %get-tuple-element.23, bf16[1,4,3072]{2,1,0:T(4,128)(2,1)S(1)} %copy-done.1, bf16[1,4,3072]{2,1,0:T(4,128)(2,1)S(1)} %copy-done.2, f32[4,24]{0,1:T(8,128)S(1)} %get-tuple-element.21), kind=kOutput, calls=%fused_computation.11 | convolution fusion | flops 19685376 | bytes 3195360 | tf_op jit(solution)/shard_map/bphd,bphe->bhde/dot_general | solution.py:51
  35.5 0.1 subtract_maximum_fusion
  35.5 0.0 all-to-all-done
  35.6 0.2 slice_reduce_fusion
  35.8 0.1 fusion.47
  35.9 0.1 subtract_bitcast_fusion
  36.0 2.9 %fusion.17 = f32[1,4,24,128]{3,1,2,0:T(4,128)S(1)} fusion(f32[1,24,128,128]{3,2,1,0:T(8,128)} %bitcast_add_fusion, f32[4,24]{0,1:T(8,128)S(1)} %get-tuple-element.20, f32[1,4,24,64]{3,1,2,0:T(4,128)S(1)} %get-tuple-element.14, f32[1,4,24,64]{3,1,2,0:T(4,128)S(1)} %get-tuple-element.15), kind=kOutput, calls=%fused_computation.17 | convolution fusion | flops 18898944 | bytes 1671552 | tf_op jit(solution)/shard_map/bihd,bhde->bihe/dot_general | solution.py:69
  38.8 0.4 convolution_multiply_fusion
  39.2 0.3 fusion.51
  39.5 0.2 multiply_reduce_fusion
  39.7 0.1 fusion.37
  39.8 14.5 %all-gather = bf16[8,4,3072]{2,1,0:T(4,128)(2,1)S(1)} all-gather(bf16[1,4,3072]{2,1,0:T(4,128)(2,1)S(1)} %fusion.37), channel_id=1, replica_groups=mesh['dp'=4,'kv'=4,'tp'=2] {'kv','tp'}, dimensions={0}, use_global_device_ids=true | all-gather | bytes 221184 | tf_op jit(solution)/shard_map/all_gather | solution.py:126
  54.4 1.3 %convolution_convert_fusion = bf16[32,512]{1,0:T(8,128)(2,1)} fusion(bf16[32,3072]{1,0:T(8,128)(2,1)S(1)} %reshape.491, bf16[3072,512]{1,0:T(8,128)(2,1)S(1)} %copy-done), kind=kOutput, calls=%fused_computation.13 | convolution fusion | flops 100679680 | bytes 3375104 | tf_op jit(solution)/shard_map/dot_general | solution.py:125
  (12 shorter events, 0.1 us)
Async XLA Ops:
  0.6 53.8 %copy-start = (bf16[3072,512]{1,0:T(8,128)(2,1)S(1)}, bf16[3072,512]{1,0:T(8,128)(2,1)}, u32[]{:S(2)}) copy-start(bf16[3072,512]{1,0:T(8,128)(2,1)} %param.20) | copy-start | bytes 9437188
  16.9 13.2 %copy-start.3 = (f32[24]{0:T(128)S(1)}, f32[24]{0:T(128)}, u32[]{:S(2)}) copy-start(f32[24]{0:T(128)} %param.21) | copy-start | bytes 292
  16.9 13.3 %copy-start.4 = (s32[1,4]{1,0:T(1,128)S(1)}, s32[1,4]{1,0:T(1,128)}, u32[]{:S(2)}) copy-start(s32[1,4]{1,0:T(1,128)} %param.26) | copy-start | bytes 52
  17.0 14.3 %copy-start.1 = (bf16[1,4,3072]{2,1,0:T(4,128)(2,1)S(1)}, bf16[1,4,3072]{2,1,0:T(4,128)(2,1)}, u32[]{:S(2)}) copy-start(bf16[1,4,3072]{2,1,0:T(4,128)(2,1)} %param.23) | copy-start | bytes 73732
  17.0 14.3 %copy-start.2 = (bf16[1,4,3072]{2,1,0:T(4,128)(2,1)S(1)}, bf16[1,4,3072]{2,1,0:T(4,128)(2,1)}, u32[]{:S(2)}) copy-start(bf16[1,4,3072]{2,1,0:T(4,128)(2,1)} %param.24) | copy-start | bytes 73732
  24.0 11.6 %all-to-all-start = ((bf16[32,4,384]{2,1,0:T(4,128)(2,1)}), bf16[32,4,384]{2,1,0:T(4,128)(2,1)S(1)}, u32[]{:S(2)}, u32[]{:S(2)}) async-start(bf16[32,4,384]{2,1,0:T(4,128)(2,1)} %reshape.477), calls=%async_computation | async-start | bytes 196608 | tf_op jit(solution)/shard_map/all_to_all | solution.py:104
where the time goes:
time: 56.1 us; the launch traced here: 55.6 us
  blocking collectives  30.6 us (55%)
  matrix products  16.1 us (29%)
  starting transfers between devices  4.84 us (9%)
  between operations  2.12 us (4%)
  other arithmetic  1.07 us (2%)
  local copies, waits for them, and re-layouts  0.95 us (2%)
    all_gather x1, blocking collectives, per_device(): lax.all_gather(tokens, ('kv', 'tp'), axis=1, tiled=True).astype(jnp.float32)  16.1 us
    all_gather x1, blocking collectives, per_device(): lax.all_gather(mixed, ('kv', 'tp'), axis=0, tiled=True)  14.5 us
    dot_general x1, matrix products, per_device(): jnp.dot(full_normed, weights, preferred_element_type=jnp.float32)  6.34 us
    all_to_all x1, starting transfers between devices, per_device(): lax.all_to_all(projected, ('kv', 'tp'), split_axis=0, concat_axis=2, tile...  4.84 us
    dot_general x1, matrix products, advance(): jnp.einsum('bphd,bphe->bhde', old_keys * weights[..., None], old_values,...  4.16 us
    dot_general x1, matrix products, retain(): jnp.einsum('bihd,bhde->bihe', rotated_q, carried, precision=HIGH)  2.85 us
    dot_general x1, matrix products, per_device(): jnp.dot(lax.all_gather(mixed, ('kv', 'tp'), axis=0, tiled=True), w_output...  1.26 us
  transfers between devices with their start and end apart: 1, of which 0 were waited for; matrix products, arithmetic and copies ran while one was open for 10% of the time, Pallas kernels for 0%

commit v1 on v0

--- a/solution.py
+++ b/solution.py
@@ -1,6 +1,11 @@
+import functools
+
 import jax
 import jax.numpy as jnp
+import numpy as np
 from jax import lax
+from jax.experimental import pallas as pl
+from jax.experimental.pallas import tpu as pltpu
 from jax.sharding import PartitionSpec as P
 
 EPS = 1e-06
@@ -130,6 +135,441 @@
     return (output, carried)
 
 
+MESH = pl.DeviceIdType.MESH
+
+
+def cos_sin(angles):
+    quarter = jnp.floor(angles * (2.0 / np.pi) + 0.5)
+    rest = angles - quarter * 1.5703125
+    rest = rest - quarter * 4.8375129699707031e-4
+    rest = rest - quarter * 7.549789948768648e-8
+    sq = rest * rest
+    sine = rest + rest * sq * (-1.6666654611e-1 + sq * (8.3321608736e-3 - sq * 1.9515295891e-4))
+    cosine = 1.0 - 0.5 * sq + sq * sq * (
+        4.166664568298827e-2 + sq * (-1.388731625493765e-3 + sq * 2.443315711809948e-5)
+    )
+    which = quarter.astype(jnp.int32)
+    swap = (which & 1) == 1
+    sin_out = jnp.where(swap, cosine, sine)
+    cos_out = jnp.where(swap, sine, cosine)
+    sin_out = jnp.where((which & 2) == 2, -sin_out, sin_out)
+    cos_out = jnp.where(((which + 1) & 2) == 2, -cos_out, cos_out)
+    return cos_out, sin_out
+
+
+def swap_rows(x):
+    return pltpu.roll(x, 4, axis=x.ndim - 2)
+
+
+def fused(
+    kv_size,
+    heads,
+    decay_ref,
+    accepted_ref,
+    parents_ref,
+    length_ref,
+    tokens_hbm,
+    gain_hbm,
+    freq_hbm,
+    wq_hbm,
+    wk_hbm,
+    wv_hbm,
+    wg_hbm,
+    wo_hbm,
+    state_hbm,
+    pk_hbm,
+    pv_hbm,
+    out_hbm,
+    carried_hbm,
+    xg,
+    gain,
+    freq,
+    w_all,
+    w_out,
+    state,
+    pk,
+    pv,
+    carried,
+    split,
+    dtab,
+    stab,
+    stage,
+    recvq,
+    msend,
+    mg,
+    lhs,
+    outb,
+    local_sem,
+    w_sem,
+    x_send,
+    x_recv,
+    p_send,
+    p_recv,
+    m_send,
+    m_recv,
+):
+    n = kv_size * 2
+    kv, tp = lax.axis_index("kv"), lax.axis_index("tp")
+    me = kv * 2 + tp
+    block = xg.shape[2]
+    cols = wq_hbm.shape[1]
+    per = cols // 128
+
+    def owner(dz, dt):
+        return lax.rem(kv - dz + kv_size, kv_size) * 2 + (1 - tp if dt else tp)
+
+    def target(dz, dt):
+        return {"kv": lax.rem(kv + dz, kv_size), "tp": 1 - tp if dt else tp}
+
+    near = sorted(range(1, kv_size), key=lambda d: min(d, kv_size - d))
+    far = near[::-1]
+    order = [(0, 0), (0, 1)] + [(d, 0) for d in near] + [(d, 1) for d in near]
+
+    def local(src, dst, i):
+        return pltpu.make_async_copy(src, dst, local_sem.at[i])
+
+    tok_copy = local(tokens_hbm, xg.at[me], 0)
+    tok_copy.start()
+    small = [
+        local(gain_hbm, gain, 1),
+        local(freq_hbm, freq, 2),
+        local(pk_hbm, pk, 3),
+        local(pv_hbm, pv, 4),
+        local(state_hbm, state, 5),
+    ]
+    for c in small:
+        c.start()
+    barrier = pltpu.get_barrier_semaphore()
+    for dz in range(kv_size):
+        for dt in range(2):
+            if dz or dt:
+                pl.semaphore_signal(barrier, inc=1, device_id=target(dz, dt), device_id_type=MESH)
+    w_copies = []
+    for t, (dz, dt) in enumerate(order):
+        rows = pl.ds(pl.multiple_of(owner(dz, dt) * block, block), block)
+        these = []
+        for r, ref in enumerate((wq_hbm, wk_hbm, wv_hbm, wg_hbm)):
+            c = pltpu.make_async_copy(
+                ref.at[rows], w_all.at[rows, pl.ds(r * cols, cols)], w_sem.at[t, r]
+            )
+            c.start()
+            these.append(c)
+        w_copies.append(these)
+    wo_copy = local(wo_hbm, w_out, 6)
+    wo_copy.start()
+
+    def gather_start(buf, send_sem, recv_sem):
+        sends = {}
+        for dz in far:
+            sends[dz, 0] = pltpu.make_async_remote_copy(
+                src_ref=buf.at[me], dst_ref=buf.at[me], send_sem=send_sem.at[dz],
+                recv_sem=recv_sem.at[dz], device_id=target(dz, 0), device_id_type=MESH,
+            )
+        sends[0, 1] = pltpu.make_async_remote_copy(
+            src_ref=buf.at[me], dst_ref=buf.at[me], send_sem=send_sem.at[kv_size],
+            recv_sem=recv_sem.at[kv_size], device_id=target(0, 1), device_id_type=MESH,
+        )
+        for c in sends.values():
+            c.start()
+        return sends
+
+    def relay(buf, send_sem, recv_sem, dz):
+        slot = buf.at[owner(dz, 0)]
+        c = pltpu.make_async_remote_copy(
+            src_ref=slot, dst_ref=slot, send_sem=send_sem.at[kv_size + dz],
+            recv_sem=recv_sem.at[kv_size + dz], device_id=target(0, 1), device_id_type=MESH,
+        )
+        c.start()
+        return c
+
+    def arrived(buf, send_sem, recv_sem, dz, dt):
+        slot = buf.at[owner(dz, dt)]
+        i = dz + dt * kv_size
+        pltpu.make_async_remote_copy(
+            src_ref=slot, dst_ref=slot, send_sem=send_sem.at[i], recv_sem=recv_sem.at[i],
+            device_id=target(0, 1), device_id_type=MESH,
+        ).wait_recv()
+
+    tok_copy.wait()
+    pl.semaphore_wait(barrier, n - 1)
+    x_sends = gather_start(xg, x_send, x_recv)
+
+    row = lax.broadcasted_iota(jnp.int32, (8, 128), 0)
+    lane = lax.broadcasted_iota(jnp.int32, (8, 128), 1)
+    which = row & 3
+    low = row < 4
+    props = 4
+    parent = [parents_ref[0, i] for i in range(props)]
+    anc = [[jnp.int32(1 if i == j else 0) for j in range(props)] for i in range(props)]
+    depth = [jnp.int32(0) for i in range(props)]
+    for i in range(1, props):
+        for j in range(i):
+            hit = jnp.where(parent[i] == j, jnp.int32(1), jnp.int32(0))
+            depth[i] = depth[i] + hit * (depth[j] + 1)
+            for m in range(i):
+                anc[i][m] = anc[i][m] + hit * anc[j][m]
+
+    def by_row(values):
+        out = jnp.full((8, 128), values[0], jnp.int32)
+        for i in range(1, props):
+            out = jnp.where(which == i, jnp.full((8, 128), values[i], jnp.int32), out)
+        return out.astype(jnp.float32)
+
+    deep = by_row(depth)
+    acc_count = jnp.full((8, 128), accepted_ref[0], jnp.int32).astype(jnp.float32)
+    base = jnp.full((8, 128), accepted_ref[0] + length_ref[0], jnp.int32).astype(jnp.float32)
+    index = which.astype(jnp.float32)
+    age = jnp.maximum(acc_count - 1.0 - index, 0.0)
+    live = jnp.where(index < acc_count, 1.0, 0.0)
+    spacing = [jnp.maximum(deep - depth[j].astype(jnp.float32), 0.0) for j in range(props)]
+    kin = [jnp.where(low, by_row([anc[i][j] for i in range(props)]), 0.0) for j in range(props)]
+
+    for c in small:
+        c.wait()
+    cosine, sine = cos_sin((base + deep) * freq[...])
+    row_scale = jnp.where(low, 1.0, 128.0 ** -0.5)
+    cos_t = cosine * row_scale
+    sin_t = jnp.where(lane < 64, -sine, sine) * row_scale
+
+    def advance_head(h, carry):
+        rate = jnp.full((8, 128), decay_ref[h], jnp.float32)
+        for j in range(props):
+            dtab[h, j] = kin[j] * jnp.exp(-rate * spacing[j])
+        stab[h] = jnp.exp(-rate * (deep + 1.0))
+        at = pl.ds(pl.multiple_of(h * 128, 128), 128)
+        kh = pk[0, :, at].astype(jnp.float32)
+        vh = pv[0, :, at].astype(jnp.float32)
+        weighted = jnp.concatenate([kh, kh], axis=0) * (live * jnp.exp(-rate * age))
+        upper = weighted.astype(jnp.bfloat16).astype(jnp.float32)
+        both = jnp.where(low, upper, weighted - upper)
+        v2 = jnp.concatenate([vh, vh], axis=0).astype(jnp.bfloat16)
+        added = lax.dot_general(
+            both.T.astype(jnp.bfloat16), v2, (((1,), (0,)), ((), ())),
+            preferred_element_type=jnp.float32,
+        )
+        kept = jnp.exp(-rate * acc_count)[0:1]
+        new = kept * state[0, h] + added
+        carried[0, h] = new
+        big = new.astype(jnp.bfloat16)
+        split[h, :, 0:128] = big
+        split[h, :, 128:256] = (new - big.astype(jnp.float32)).astype(jnp.bfloat16)
+        return carry
+
+    lax.fori_loop(0, heads, advance_head, 0, unroll=2)
+
+    squares = jnp.zeros((xg.shape[1], 128), jnp.float32)
+    total = None
+
+    def project(total, squares, t, dz, dt):
+        who = owner(dz, dt)
+        for c in w_copies[t]:
+            c.wait()
+        x = xg[who].astype(jnp.float32)
+        for q in range(block // 128):
+            part = x[:, q * 128:(q + 1) * 128]
+            squares = squares + part * part
+        at = pl.ds(pl.multiple_of(who * block, block), block)
+        xn = (x * gain[:, at]).astype(jnp.bfloat16)
+        y = jnp.dot(xn, w_all[at, :], preferred_element_type=jnp.float32)
+        return (y if total is None else total + y), squares
+
+    total, squares = project(total, squares, 0, 0, 0)
+    arrived(xg, x_send, x_recv, 0, 1)
+    total, squares = project(total, squares, 1, 0, 1)
+    relays = []
+    waited = set()
+    for t, (dz, dt) in enumerate(order):
+        if t < 2:
+            continue
+        if dt == 0:
+            for d in (near[:2] if dz in near[:2] else [dz]):
+                if d not in waited:
+                    waited.add(d)
+                    arrived(xg, x_send, x_recv, d, 0)
+                    relays.append(relay(xg, x_send, x_recv, d))
+        else:
+            arrived(xg, x_send, x_recv, dz, 1)
+        total, squares = project(total, squares, t, dz, dt)
+    width = block * n
+    scale = lax.rsqrt(jnp.sum(squares, axis=1, keepdims=True) * (1.0 / width) + EPS)
+    total = total * scale
+    low_c = lax.broadcasted_iota(jnp.int32, (8, cols), 0) < 4
+    for t in range(n // 2):
+        q, k, v, g = [total[8 * t:8 * t + 8, r * cols:(r + 1) * cols] for r in range(4)]
+        stage[2 * t] = jnp.concatenate(
+            [jnp.where(low_c, q, swap_rows(k)), jnp.where(low_c, v, swap_rows(g))], axis=0
+        ).astype(jnp.bfloat16)
+        stage[2 * t + 1] = jnp.concatenate(
+            [jnp.where(low_c, swap_rows(q), k), jnp.where(low_c, swap_rows(v), g)], axis=0
+        ).astype(jnp.bfloat16)
+    p_sends = []
+    for dz in far + [0]:
+        for dt in range(2):
+            if dz or dt:
+                to = target(dz, dt)
+                c = pltpu.make_async_remote_copy(
+                    src_ref=stage.at[to["kv"] * 2 + to["tp"]], dst_ref=recvq.at[me],
+                    send_sem=p_send.at[dz * 2 + dt], recv_sem=p_recv.at[dz * 2 + dt],
+                    device_id=to, device_id_type=MESH,
+                )
+                c.start()
+                p_sends.append(c)
+    recvq[me] = stage[me]
+    carried_copy = local(carried, carried_hbm, 7)
+    carried_copy.start()
+    wo_copy.wait()
+    for dz in range(kv_size):
+        for dt in range(2):
+            if dz or dt:
+                slot = recvq.at[owner(dz, dt)]
+                i = dz * 2 + dt
+                pltpu.make_async_remote_copy(
+                    src_ref=slot, dst_ref=slot, send_sem=p_send.at[i], recv_sem=p_recv.at[i],
+                    device_id=target(0, 1), device_id_type=MESH,
+                ).wait_recv()
+
+    low3 = low[None]
+    for k in range(per):
+        got = recvq[:, :, k * 128:(k + 1) * 128].astype(jnp.float32)
+        qk, vg = got[:, 0:8], got[:, 8:16]
+        turned = qk * cos_t[None] + pltpu.roll(qk, 64, axis=2) * sin_t[None]
+        mine = [dtab[s * per + k] for s in range(n)]
+        decay = jnp.stack([stab[s * per + k] for s in range(n)])
+        qs = turned * decay
+        qs = jnp.where(low3, qs, swap_rows(qs))
+        upper = qs.astype(jnp.bfloat16).astype(jnp.float32)
+        pair = jnp.where(low3, upper, qs - upper).astype(jnp.bfloat16)
+        raws = []
+        for s in range(n):
+            y = jnp.dot(pair[s], split[s * per + k], preferred_element_type=jnp.float32)
+            raws.append(y[:, 0:128] + y[:, 128:256])
+        raw = jnp.stack(raws)
+        raw = raw + swap_rows(raw)
+        for j in range(props):
+            score = jnp.sum(turned * turned[:, 4 + j:5 + j, :], axis=2, keepdims=True)
+            raw = raw + score * jnp.stack([m[j] for m in mine]) * vg[:, j:j + 1, :]
+        centred = raw - jnp.sum(raw, axis=2, keepdims=True) * (1.0 / 128)
+        spread = jnp.sum(centred * centred, axis=2, keepdims=True) * (1.0 / 128)
+        gate = swap_rows(vg)
+        mixed = centred * lax.rsqrt(spread + EPS) * (gate / (1.0 + jnp.exp(-gate)))
+        group = n // 4
+        for b in range(group):
+            first = jnp.where(low, mixed[b], swap_rows(mixed[group + b]))
+            second = jnp.where(low, mixed[2 * group + b], swap_rows(mixed[3 * group + b]))
+            at = b * cols + k * 128
+            mg[me, :, at:at + 128] = jnp.concatenate([first, second], axis=0).astype(jnp.bfloat16)
+
+    m_sends = gather_start(mg, m_send, m_recv)
+    m_relays = []
+    for dz in near:
+        arrived(mg, m_send, m_recv, dz, 0)
+        m_relays.append(relay(mg, m_send, m_recv, dz))
+    arrived(mg, m_send, m_recv, 0, 1)
+    for dz in near:
+        arrived(mg, m_send, m_recv, dz, 1)
+    chunk = mg.shape[2]
+    low_m = lax.broadcasted_iota(jnp.int32, (8, chunk), 0) < 4
+    for t in range(n // 2):
+        one = mg[2 * t].astype(jnp.float32)
+        two = mg[2 * t + 1].astype(jnp.float32)
+        for c in range(4):
+            at = 8 * (c // 2)
+            a, b = one[at:at + 8], two[at:at + 8]
+            if c % 2 == 0:
+                piece = jnp.where(low_m, a, swap_rows(b))
+            else:
+                piece = jnp.where(low_m, swap_rows(a), b)
+            lhs[8 * t:8 * t + 8, c * chunk:(c + 1) * chunk] = piece
+    outb[...] = jnp.dot(
+        lhs[...].astype(jnp.bfloat16), w_out[...], preferred_element_type=jnp.float32
+    ).astype(jnp.bfloat16)
+    out_copy = local(outb, out_hbm, 8)
+    out_copy.start()
+    for c in list(x_sends.values()) + relays + p_sends + list(m_sends.values()) + m_relays:
+        c.wait_send()
+    carried_copy.wait()
+    out_copy.wait()
+
+
+def fused_device(
+    kv_size, tokens, norm_gain, w_query, w_key, w_value, w_gate, w_output, decay_rate, state,
+    prev_keys, prev_values, accepted, parents, seq_length,
+):
+    n = kv_size * 2
+    rows, block = tokens.shape
+    width, cols = w_query.shape
+    heads = decay_rate.shape[0]
+    hid, out_cols = w_output.shape
+    freq = 10000.0 ** (-(np.arange(128) % 64) / 64.0)
+    freq = jnp.asarray(freq.astype(np.float32)[None, :])
+    smem = pl.BlockSpec(memory_space=pltpu.SMEM)
+    hbm = pl.BlockSpec(memory_space=pl.ANY)
+    bf, f32 = jnp.bfloat16, jnp.float32
+    dma = pltpu.SemaphoreType.DMA
+    return pl.pallas_call(
+        functools.partial(fused, kv_size, heads),
+        out_shape=(
+            jax.ShapeDtypeStruct((rows, out_cols), bf),
+            jax.ShapeDtypeStruct(state.shape, f32),
+        ),
+        in_specs=[smem] * 4 + [hbm] * 11,
+        out_specs=(hbm, hbm),
+        scratch_shapes=[
+            pltpu.VMEM((n, rows, block), bf),
+            pltpu.VMEM((1, width), f32),
+            pltpu.VMEM((1, 128), f32),
+            pltpu.VMEM((width, 4 * cols), bf),
+            pltpu.VMEM((hid, out_cols), bf),
+            pltpu.VMEM(state.shape, f32),
+            pltpu.VMEM(prev_keys.shape, bf),
+            pltpu.VMEM(prev_values.shape, bf),
+            pltpu.VMEM(state.shape, f32),
+            pltpu.VMEM((heads, 128, 256), bf),
+            pltpu.VMEM((heads, 4, 8, 128), f32),
+            pltpu.VMEM((heads, 8, 128), f32),
+            pltpu.VMEM((n, 16, cols), bf),
+            pltpu.VMEM((n, 16, cols), bf),
+            pltpu.VMEM((16, hid // 4), bf),
+            pltpu.VMEM((n, 16, hid // 4), bf),
+            pltpu.VMEM((rows, hid), f32),
+            pltpu.VMEM((rows, out_cols), bf),
+            dma((9,)),
+            dma((n, 4)),
+            dma((n,)),
+            dma((n,)),
+            dma((n,)),
+            dma((n,)),
+            dma((n,)),
+            dma((n,)),
+        ],
+        compiler_params=pltpu.CompilerParams(
+            collective_id=0, has_side_effects=True, vmem_limit_bytes=60 * 1024 * 1024
+        ),
+    )(
+        decay_rate, accepted, parents, seq_length, tokens, norm_gain[None, :], freq, w_query,
+        w_key, w_value, w_gate, w_output, state, prev_keys, prev_values,
+    )
+
+
+def choose(kv_size, tp_size, *args):
+    tokens, w_query, state, parents = args[0], args[2], args[8], args[12]
+    n = kv_size * tp_size
+    fits = (
+        tp_size == 2
+        and n % 4 == 0
+        and kv_size > 2
+        and state.shape[0] == 1
+        and state.shape[2:] == (128, 128)
+        and parents.shape[1] == 4
+        and w_query.shape[1] % 128 == 0
+        and tokens.shape[0] == 4 * n
+        and tokens.shape[1] % 128 == 0
+    )
+    if fits:
+        return fused_device(kv_size, *args)
+    return per_device(*args)
+
+
 def solution(mesh):
     placed = (
         P("dp", ("kv", "tp")),
@@ -148,7 +588,7 @@
         P(("dp", "kv", "tp")),
     )
     return jax.shard_map(
-        per_device,
+        functools.partial(choose, mesh.shape["kv"], mesh.shape["tp"]),
         mesh=mesh,
         in_specs=placed,
         out_specs=(P("dp", ("kv", "tp")), P(("dp", "kv", "tp"), None, None, None)),

time: 56.1 us -> 30 us (0.53)
  blocking collectives: 30.6 us -> 0 us
  Pallas kernels: 0 us -> 23.7 us
  matrix products: 16.1 us -> 0 us
  starting transfers between devices: 4.84 us -> 0 us
  local copies, waits for them, and re-layouts: 0.95 us -> 4.08 us
  other arithmetic: 1.07 us -> 0 us
    all_gather x2 -> x0, blocking collectives: 30.6 us -> none  [the longest x1 16.1 us: per_device(): lax.all_gather(tokens, ('kv', 'tp'), axis=1, tiled=True).astype(jnp.float32)]
    pallas_call x0 -> x1, Pallas kernels: none -> 23.7 us  [fused_device(): pl.pallas_call(functools.partial(fused, kv_size, heads), out_shape=(jax.S...]
    dot_general x9 -> x0, matrix products: 16.1 us -> none  [the longest x1 6.34 us: per_device(): jnp.dot(full_normed, weights, preferred_element_type=jnp.float32)]
    all_to_all x1 -> x0, starting transfers between devices: 4.84 us -> none  [per_device(): lax.all_to_all(projected, ('kv', 'tp'), split_axis=0, concat_axis=2, tile...]
    unnamed x11 -> x2, local copies, waits for them, and re-layouts: 0.08 us -> 4.08 us
    reshape x1 -> x0, local copies, waits for them, and re-layouts: 0.65 us -> none  [per_device(): projected.astype(jnp.bfloat16).reshape(rows_count, 4, columns // 4)]
  transfers between devices with their start and end apart: 1 -> 0, of which waited for: 0 -> 0; matrix products, arithmetic and copies ran while one was open for 10% -> 0% of each run, Pallas kernels for 0% -> 0%
where the time goes in v1:
time: 30 us; the launch traced here: 29.7 us
  Pallas kernels  23.7 us (79%)
  local copies, waits for them, and re-layouts  4.08 us (14%)
  between operations  1.94 us (6%)
    pallas_call x1, Pallas kernels, fused_device(): pl.pallas_call(functools.partial(fused, kv_size, heads), out_shape=(jax.S...  23.7 us
    unnamed x2, local copies, waits for them, and re-layouts  4.08 us

profile of v1, /device:TPU:1, one launch (start us, length us, event | category | flops | bytes accessed | tf_op | source)
XLA Modules:
  0.0 29.7 jit_solution(14399450071725615664)
XLA Ops:
  1.9 23.7 %shard_map.158 = (bf16[32,512]{1,0:T(8,128)(2,1)}, f32[1,24,128,128]{3,2,1,0:T(8,128)}) custom-call(f32[24]{0:T(128)} %decay_ref.1, s32[1]{0:T(128)S(6)} %copy.19.accepted_ref, s32[1,4]{1,0:T(1,128)} %parents_ref.1, s32[1]{0:T(128)S(6)} %copy.20.length_ref, bf16[32,512]{1,0:T(8,128)(2,1)} %tokens_hbm.1, f32[1,4096]{1,0:T(1,128)} %bitcast.1, ...), custom_call_target="tpu_custom_call" | custom-call | tf_op jit(solution)/shard_map/pallas_call | solution.py:509
  25.7 1.4 %copy.21 = bf16[32,512]{1,0:T(8,128)(2,1)} copy(bf16[32,512]{1,0:T(8,128)(2,1)} %get-tuple-element.4) | data formatting | bytes 65536
  27.0 2.7 %copy.22 = f32[1,24,128,128]{3,2,1,0:T(8,128)} copy(f32[1,24,128,128]{3,2,1,0:T(8,128)} %get-tuple-element.5) | data formatting | bytes 3145728

commit v2 on v1

--- a/solution.py
+++ b/solution.py
@@ -164,10 +164,10 @@
 def fused(
     kv_size,
     heads,
-    decay_ref,
-    accepted_ref,
-    parents_ref,
-    length_ref,
+    decay_hbm,
+    accepted_hbm,
+    parents_hbm,
+    length_hbm,
     tokens_hbm,
     gain_hbm,
     freq_hbm,
@@ -179,26 +179,25 @@
     state_hbm,
     pk_hbm,
     pv_hbm,
-    out_hbm,
-    carried_hbm,
+    mg,
+    carried,
+    w_out,
     xg,
     gain,
     freq,
     w_all,
-    w_out,
     state,
     pk,
     pv,
-    carried,
     split,
     dtab,
     stab,
     stage,
     recvq,
-    msend,
-    mg,
-    lhs,
-    outb,
+    decay_ref,
+    accepted_ref,
+    parents_ref,
+    length_ref,
     local_sem,
     w_sem,
     x_send,
@@ -215,35 +214,48 @@
     cols = wq_hbm.shape[1]
     per = cols // 128
 
-    def owner(dz, dt):
-        return lax.rem(kv - dz + kv_size, kv_size) * 2 + (1 - tp if dt else tp)
-
-    def target(dz, dt):
-        return {"kv": lax.rem(kv + dz, kv_size), "tp": 1 - tp if dt else tp}
-
-    near = sorted(range(1, kv_size), key=lambda d: min(d, kv_size - d))
+    ranked = [sorted(range(kv_size), key=lambda o: abs(o - z)) for z in range(kv_size)]
+    seat = [
+        sum(jnp.where(kv == z, ranked[z][d], 0) for z in range(kv_size)) for d in range(kv_size)
+    ]
+
+    def owner(d, dt):
+        return seat[d] * 2 + (1 - tp if dt else tp)
+
+    def target(d, dt):
+        return {"kv": seat[d], "tp": 1 - tp if dt else tp}
+
+    near = list(range(1, kv_size))
     far = near[::-1]
     order = [(0, 0), (0, 1)] + [(d, 0) for d in near] + [(d, 1) for d in near]
 
     def local(src, dst, i):
         return pltpu.make_async_copy(src, dst, local_sem.at[i])
 
+    barrier = pltpu.get_barrier_semaphore()
+    for dz in range(kv_size):
+        for dt in range(2):
+            if dz or dt:
+                pl.semaphore_signal(barrier, inc=1, device_id=target(dz, dt), device_id_type=MESH)
     tok_copy = local(tokens_hbm, xg.at[me], 0)
     tok_copy.start()
+    scalars = [
+        local(decay_hbm, decay_ref, 7),
+        local(accepted_hbm, accepted_ref, 8),
+        local(parents_hbm, parents_ref, 9),
+        local(length_hbm, length_ref, 10),
+    ]
+    for c in scalars:
+        c.start()
     small = [
         local(gain_hbm, gain, 1),
         local(freq_hbm, freq, 2),
         local(pk_hbm, pk, 3),
         local(pv_hbm, pv, 4),
-        local(state_hbm, state, 5),
     ]
     for c in small:
         c.start()
-    barrier = pltpu.get_barrier_semaphore()
-    for dz in range(kv_size):
-        for dt in range(2):
-            if dz or dt:
-                pl.semaphore_signal(barrier, inc=1, device_id=target(dz, dt), device_id_type=MESH)
+    small.append(local(state_hbm, state, 5))
     w_copies = []
     for t, (dz, dt) in enumerate(order):
         rows = pl.ds(pl.multiple_of(owner(dz, dt) * block, block), block)
@@ -252,22 +264,25 @@
             c = pltpu.make_async_copy(
                 ref.at[rows], w_all.at[rows, pl.ds(r * cols, cols)], w_sem.at[t, r]
             )
-            c.start()
             these.append(c)
         w_copies.append(these)
     wo_copy = local(wo_hbm, w_out, 6)
-    wo_copy.start()
+
+    def load(t):
+        for c in w_copies[t]:
+            c.start()
+
 
     def gather_start(buf, send_sem, recv_sem):
         sends = {}
         for dz in far:
             sends[dz, 0] = pltpu.make_async_remote_copy(
                 src_ref=buf.at[me], dst_ref=buf.at[me], send_sem=send_sem.at[dz],
-                recv_sem=recv_sem.at[dz], device_id=target(dz, 0), device_id_type=MESH,
+                recv_sem=recv_sem.at[kv], device_id=target(dz, 0), device_id_type=MESH,
             )
         sends[0, 1] = pltpu.make_async_remote_copy(
             src_ref=buf.at[me], dst_ref=buf.at[me], send_sem=send_sem.at[kv_size],
-            recv_sem=recv_sem.at[kv_size], device_id=target(0, 1), device_id_type=MESH,
+            recv_sem=recv_sem.at[kv_size + kv], device_id=target(0, 1), device_id_type=MESH,
         )
         for c in sends.values():
             c.start()
@@ -277,23 +292,30 @@
         slot = buf.at[owner(dz, 0)]
         c = pltpu.make_async_remote_copy(
             src_ref=slot, dst_ref=slot, send_sem=send_sem.at[kv_size + dz],
-            recv_sem=recv_sem.at[kv_size + dz], device_id=target(0, 1), device_id_type=MESH,
+            recv_sem=recv_sem.at[kv_size + seat[dz]], device_id=target(0, 1), device_id_type=MESH,
         )
         c.start()
         return c
 
     def arrived(buf, send_sem, recv_sem, dz, dt):
         slot = buf.at[owner(dz, dt)]
-        i = dz + dt * kv_size
+        i = seat[dz] + dt * kv_size
         pltpu.make_async_remote_copy(
             src_ref=slot, dst_ref=slot, send_sem=send_sem.at[i], recv_sem=recv_sem.at[i],
             device_id=target(0, 1), device_id_type=MESH,
         ).wait_recv()
 
     tok_copy.wait()
+    for t in range(2):
+        load(t)
     pl.semaphore_wait(barrier, n - 1)
     x_sends = gather_start(xg, x_send, x_recv)
-
+    for t in range(2, n):
+        load(t)
+    small[-1].start()
+
+    for c in scalars:
+        c.wait()
     row = lax.broadcasted_iota(jnp.int32, (8, 128), 0)
     lane = lax.broadcasted_iota(jnp.int32, (8, 128), 1)
     which = row & 3
@@ -316,46 +338,20 @@
         return out.astype(jnp.float32)
 
     deep = by_row(depth)
-    acc_count = jnp.full((8, 128), accepted_ref[0], jnp.int32).astype(jnp.float32)
-    base = jnp.full((8, 128), accepted_ref[0] + length_ref[0], jnp.int32).astype(jnp.float32)
+    acc_count = jnp.full((8, 128), accepted_ref[0, 0], jnp.int32).astype(jnp.float32)
+    base = jnp.full((8, 128), accepted_ref[0, 0] + length_ref[0, 0], jnp.int32).astype(jnp.float32)
     index = which.astype(jnp.float32)
     age = jnp.maximum(acc_count - 1.0 - index, 0.0)
     live = jnp.where(index < acc_count, 1.0, 0.0)
     spacing = [jnp.maximum(deep - depth[j].astype(jnp.float32), 0.0) for j in range(props)]
     kin = [jnp.where(low, by_row([anc[i][j] for i in range(props)]), 0.0) for j in range(props)]
 
-    for c in small:
+    for c in small[:-1]:
         c.wait()
     cosine, sine = cos_sin((base + deep) * freq[...])
     row_scale = jnp.where(low, 1.0, 128.0 ** -0.5)
     cos_t = cosine * row_scale
     sin_t = jnp.where(lane < 64, -sine, sine) * row_scale
-
-    def advance_head(h, carry):
-        rate = jnp.full((8, 128), decay_ref[h], jnp.float32)
-        for j in range(props):
-            dtab[h, j] = kin[j] * jnp.exp(-rate * spacing[j])
-        stab[h] = jnp.exp(-rate * (deep + 1.0))
-        at = pl.ds(pl.multiple_of(h * 128, 128), 128)
-        kh = pk[0, :, at].astype(jnp.float32)
-        vh = pv[0, :, at].astype(jnp.float32)
-        weighted = jnp.concatenate([kh, kh], axis=0) * (live * jnp.exp(-rate * age))
-        upper = weighted.astype(jnp.bfloat16).astype(jnp.float32)
-        both = jnp.where(low, upper, weighted - upper)
-        v2 = jnp.concatenate([vh, vh], axis=0).astype(jnp.bfloat16)
-        added = lax.dot_general(
-            both.T.astype(jnp.bfloat16), v2, (((1,), (0,)), ((), ())),
-            preferred_element_type=jnp.float32,
-        )
-        kept = jnp.exp(-rate * acc_count)[0:1]
-        new = kept * state[0, h] + added
-        carried[0, h] = new
-        big = new.astype(jnp.bfloat16)
-        split[h, :, 0:128] = big
-        split[h, :, 128:256] = (new - big.astype(jnp.float32)).astype(jnp.bfloat16)
-        return carry
-
-    lax.fori_loop(0, heads, advance_head, 0, unroll=2)
 
     squares = jnp.zeros((xg.shape[1], 128), jnp.float32)
     total = None
@@ -409,20 +405,46 @@
                 to = target(dz, dt)
                 c = pltpu.make_async_remote_copy(
                     src_ref=stage.at[to["kv"] * 2 + to["tp"]], dst_ref=recvq.at[me],
-                    send_sem=p_send.at[dz * 2 + dt], recv_sem=p_recv.at[dz * 2 + dt],
+                    send_sem=p_send.at[dz * 2 + dt], recv_sem=p_recv.at[me],
                     device_id=to, device_id_type=MESH,
                 )
                 c.start()
                 p_sends.append(c)
+    wo_copy.start()
     recvq[me] = stage[me]
-    carried_copy = local(carried, carried_hbm, 7)
-    carried_copy.start()
-    wo_copy.wait()
+    small[-1].wait()
+
+    def advance_head(h, carry):
+        rate = jnp.full((8, 128), decay_ref[h], jnp.float32)
+        for j in range(props):
+            dtab[h, j] = kin[j] * jnp.exp(-rate * spacing[j])
+        stab[h] = jnp.exp(-rate * (deep + 1.0))
+        at = pl.ds(pl.multiple_of(h * 128, 128), 128)
+        kh = pk[0, :, at].astype(jnp.float32)
+        vh = pv[0, :, at].astype(jnp.float32)
+        weighted = jnp.concatenate([kh, kh], axis=0) * (live * jnp.exp(-rate * age))
+        upper = weighted.astype(jnp.bfloat16).astype(jnp.float32)
+        both = jnp.where(low, upper, weighted - upper)
+        v2 = jnp.concatenate([vh, vh], axis=0).astype(jnp.bfloat16)
+        added = lax.dot_general(
+            both.T.astype(jnp.bfloat16), v2, (((1,), (0,)), ((), ())),
+            preferred_element_type=jnp.float32,
+        )
+        kept = jnp.exp(-rate * acc_count)[0:1]
+        new = kept * state[0, h] + added
+        carried[0, h] = new
+        big = new.astype(jnp.bfloat16)
+        split[h, :, 0:128] = big
+        split[h, :, 128:256] = (new - big.astype(jnp.float32)).astype(jnp.bfloat16)
+        return carry
+
+    lax.fori_loop(0, heads, advance_head, 0, unroll=2)
+
     for dz in range(kv_size):
         for dt in range(2):
             if dz or dt:
                 slot = recvq.at[owner(dz, dt)]
-                i = dz * 2 + dt
+                i = owner(dz, dt)
                 pltpu.make_async_remote_copy(
                     src_ref=slot, dst_ref=slot, send_sem=p_send.at[i], recv_sem=p_recv.at[i],
                     device_id=target(0, 1), device_id_type=MESH,
@@ -467,9 +489,17 @@
     arrived(mg, m_send, m_recv, 0, 1)
     for dz in near:
         arrived(mg, m_send, m_recv, dz, 1)
+    wo_copy.wait()
+    for c in list(x_sends.values()) + relays + p_sends + list(m_sends.values()) + m_relays:
+        c.wait_send()
+
+
+def finish(mg, carried, w_out, out_hbm, carried_hbm, lhs, outb, sem):
+    carried_copy = pltpu.make_async_copy(carried, carried_hbm, sem.at[0])
+    carried_copy.start()
     chunk = mg.shape[2]
     low_m = lax.broadcasted_iota(jnp.int32, (8, chunk), 0) < 4
-    for t in range(n // 2):
+    for t in range(mg.shape[0] // 2):
         one = mg[2 * t].astype(jnp.float32)
         two = mg[2 * t + 1].astype(jnp.float32)
         for c in range(4):
@@ -483,12 +513,10 @@
     outb[...] = jnp.dot(
         lhs[...].astype(jnp.bfloat16), w_out[...], preferred_element_type=jnp.float32
     ).astype(jnp.bfloat16)
-    out_copy = local(outb, out_hbm, 8)
+    out_copy = pltpu.make_async_copy(outb, out_hbm, sem.at[1])
     out_copy.start()
-    for c in list(x_sends.values()) + relays + p_sends + list(m_sends.values()) + m_relays:
-        c.wait_send()
+    out_copy.wait()
     carried_copy.wait()
-    out_copy.wait()
 
 
 def fused_device(
@@ -502,38 +530,38 @@
     hid, out_cols = w_output.shape
     freq = 10000.0 ** (-(np.arange(128) % 64) / 64.0)
     freq = jnp.asarray(freq.astype(np.float32)[None, :])
-    smem = pl.BlockSpec(memory_space=pltpu.SMEM)
-    hbm = pl.BlockSpec(memory_space=pl.ANY)
+    hbm = pl.BlockSpec(memory_space=pltpu.HBM)
+    vmem = pl.BlockSpec(memory_space=pltpu.VMEM)
     bf, f32 = jnp.bfloat16, jnp.float32
     dma = pltpu.SemaphoreType.DMA
-    return pl.pallas_call(
+    room = 67043328 - state.size * 4 - hid * out_cols * 2 - n * 16 * (hid // 4) * 2
+    gathered, new_state, w_near = pl.pallas_call(
         functools.partial(fused, kv_size, heads),
         out_shape=(
-            jax.ShapeDtypeStruct((rows, out_cols), bf),
-            jax.ShapeDtypeStruct(state.shape, f32),
+            pltpu.VMEM((n, 16, hid // 4), bf),
+            pltpu.VMEM(state.shape, f32),
+            pltpu.VMEM((hid, out_cols), bf),
         ),
-        in_specs=[smem] * 4 + [hbm] * 11,
-        out_specs=(hbm, hbm),
+        in_specs=[hbm] * 15,
+        out_specs=(vmem, vmem, vmem),
         scratch_shapes=[
             pltpu.VMEM((n, rows, block), bf),
             pltpu.VMEM((1, width), f32),
             pltpu.VMEM((1, 128), f32),
             pltpu.VMEM((width, 4 * cols), bf),
-            pltpu.VMEM((hid, out_cols), bf),
             pltpu.VMEM(state.shape, f32),
             pltpu.VMEM(prev_keys.shape, bf),
             pltpu.VMEM(prev_values.shape, bf),
-            pltpu.VMEM(state.shape, f32),
             pltpu.VMEM((heads, 128, 256), bf),
             pltpu.VMEM((heads, 4, 8, 128), f32),
             pltpu.VMEM((heads, 8, 128), f32),
             pltpu.VMEM((n, 16, cols), bf),
             pltpu.VMEM((n, 16, cols), bf),
-            pltpu.VMEM((16, hid // 4), bf),
-            pltpu.VMEM((n, 16, hid // 4), bf),
-            pltpu.VMEM((rows, hid), f32),
-            pltpu.VMEM((rows, out_cols), bf),
-            dma((9,)),
+            pltpu.SMEM(decay_rate.shape, f32),
+            pltpu.SMEM((1, 1), jnp.int32),
+            pltpu.SMEM(parents.shape, jnp.int32),
+            pltpu.SMEM((1, 1), jnp.int32),
+            dma((11,)),
             dma((n, 4)),
             dma((n,)),
             dma((n,)),
@@ -543,12 +571,27 @@
             dma((n,)),
         ],
         compiler_params=pltpu.CompilerParams(
-            collective_id=0, has_side_effects=True, vmem_limit_bytes=60 * 1024 * 1024
+            collective_id=0, has_side_effects=True, vmem_limit_bytes=room
         ),
     )(
-        decay_rate, accepted, parents, seq_length, tokens, norm_gain[None, :], freq, w_query,
+        decay_rate, accepted[None, :], parents, seq_length[None, :], tokens, norm_gain[None, :], freq, w_query,
         w_key, w_value, w_gate, w_output, state, prev_keys, prev_values,
     )
+    return pl.pallas_call(
+        finish,
+        out_shape=(
+            jax.ShapeDtypeStruct((rows, out_cols), bf),
+            jax.ShapeDtypeStruct(state.shape, f32),
+        ),
+        in_specs=[vmem] * 3,
+        out_specs=(hbm, hbm),
+        scratch_shapes=[
+            pltpu.VMEM((rows, hid), f32),
+            pltpu.VMEM((rows, out_cols), bf),
+            dma((2,)),
+        ],
+        compiler_params=pltpu.CompilerParams(vmem_limit_bytes=8 * 1024 * 1024),
+    )(gathered, new_state, w_near)
 
 
 def choose(kv_size, tp_size, *args):

time: 30 us -> 25.3 us (0.84)
  local copies, waits for them, and re-layouts: 4.08 us -> 0 us
  Pallas kernels: 23.7 us -> 23 us
    unnamed x2 -> x0, local copies, waits for them, and re-layouts: 4.08 us -> none
    pallas_call x1 -> x2, Pallas kernels: 23.7 us -> 23 us  [the longest x1 21.7 us: fused_device(): pl.pallas_call(functools.partial(fused, kv_size, heads), out_shape=(pltpu...]
where the time goes in v2:
time: 25.3 us; the launch traced here: 25 us
  Pallas kernels  23 us (91%)
  between operations  1.94 us (8%)
    pallas_call x1, Pallas kernels, fused_device(): pl.pallas_call(functools.partial(fused, kv_size, heads), out_shape=(pltpu...  21.7 us
    pallas_call x1, Pallas kernels, fused_device(): pl.pallas_call(finish, out_shape=(jax.ShapeDtypeStruct((rows, out_cols),...  1.28 us

profile of v2, /device:TPU:1, one launch (start us, length us, event | category | flops | bytes accessed | tf_op | source)
XLA Modules:
  0.0 25.0 jit_solution(4033068795894308087)
XLA Ops:
  1.9 21.7 %shard_map.158 = (bf16[8,16,768]{2,1,0:T(8,128)(2,1)S(1)}, f32[1,24,128,128]{3,2,1,0:T(8,128)S(1)}, bf16[3072,512]{1,0:T(8,128)(2,1)S(1)}) custom-call(f32[24]{0:T(128)} %decay_hbm.1, s32[1,1]{1,0:T(1,128)} %bitcast.3.accepted_hbm, s32[1,4]{1,0:T(1,128)} %parents_hbm.1, s32[1,1]{1,0:T(1,128)} %bitcast.4.length_hbm, bf16[32,512]{1,0:T(8,128)(2,1)} %tokens_hbm.1, ...), custom_call_target="tpu_custom_call" | custom-call | tf_op jit(solution)/shard_map/pallas_call | solution.py:538
  23.7 1.3 %shard_map.159 = (bf16[32,512]{1,0:T(8,128)(2,1)}, f32[1,24,128,128]{3,2,1,0:T(8,128)}) custom-call(bf16[8,16,768]{2,1,0:T(8,128)(2,1)S(1)} %get-tuple-element.5.mg, f32[1,24,128,128]{3,2,1,0:T(8,128)S(1)} %get-tuple-element.6.carried, bf16[3072,512]{1,0:T(8,128)(2,1)S(1)} %get-tuple-element.7.w_out), custom_call_target="tpu_custom_call" | custom-call | tf_op jit(solution)/shard_map/pallas_call | solution.py:580

commit v3 on v2

--- a/solution.py
+++ b/solution.py
@@ -495,8 +495,15 @@
 
 
 def finish(mg, carried, w_out, out_hbm, carried_hbm, lhs, outb, sem):
-    carried_copy = pltpu.make_async_copy(carried, carried_hbm, sem.at[0])
-    carried_copy.start()
+    heads = carried.shape[1]
+    pieces = 8 if heads % 8 == 0 else 1
+    count = heads // pieces
+    carried_copies = []
+    for i in range(pieces):
+        at = pl.ds(i * count, count)
+        c = pltpu.make_async_copy(carried.at[:, at], carried_hbm.at[:, at], sem.at[i])
+        c.start()
+        carried_copies.append(c)
     chunk = mg.shape[2]
     low_m = lax.broadcasted_iota(jnp.int32, (8, chunk), 0) < 4
     for t in range(mg.shape[0] // 2):
@@ -513,10 +520,11 @@
     outb[...] = jnp.dot(
         lhs[...].astype(jnp.bfloat16), w_out[...], preferred_element_type=jnp.float32
     ).astype(jnp.bfloat16)
-    out_copy = pltpu.make_async_copy(outb, out_hbm, sem.at[1])
+    out_copy = pltpu.make_async_copy(outb, out_hbm, sem.at[8])
     out_copy.start()
     out_copy.wait()
-    carried_copy.wait()
+    for c in carried_copies:
+        c.wait()
 
 
 def fused_device(
@@ -588,7 +596,7 @@
         scratch_shapes=[
             pltpu.VMEM((rows, hid), f32),
             pltpu.VMEM((rows, out_cols), bf),
-            dma((2,)),
+            dma((9,)),
         ],
         compiler_params=pltpu.CompilerParams(vmem_limit_bytes=8 * 1024 * 1024),
     )(gathered, new_state, w_near)

time: 25.3 us -> 25.5 us (level)
  no operation moved by 1% of the time
where the time goes in v3:
time: 25.5 us; the launch traced here: 25.2 us
  Pallas kernels  23.2 us (91%)
  between operations  1.94 us (8%)
    pallas_call x1, Pallas kernels, fused_device(): pl.pallas_call(functools.partial(fused, kv_size, heads), out_shape=(pltpu...  21.7 us
    pallas_call x1, Pallas kernels, fused_device(): pl.pallas_call(finish, out_shape=(jax.ShapeDtypeStruct((rows, out_cols),...  1.48 us

profile of v3, /device:TPU:1, one launch (start us, length us, event | category | flops | bytes accessed | tf_op | source)
XLA Modules:
  0.0 25.2 jit_solution(14079202874673717391)
XLA Ops:
  1.9 21.7 %shard_map.158 = (bf16[8,16,768]{2,1,0:T(8,128)(2,1)S(1)}, f32[1,24,128,128]{3,2,1,0:T(8,128)S(1)}, bf16[3072,512]{1,0:T(8,128)(2,1)S(1)}) custom-call(f32[24]{0:T(128)} %decay_hbm.1, s32[1,1]{1,0:T(1,128)} %bitcast.3.accepted_hbm, s32[1,4]{1,0:T(1,128)} %parents_hbm.1, s32[1,1]{1,0:T(1,128)} %bitcast.4.length_hbm, bf16[32,512]{1,0:T(8,128)(2,1)} %tokens_hbm.1, ...), custom_call_target="tpu_custom_call" | custom-call | tf_op jit(solution)/shard_map/pallas_call | solution.py:546
  23.7 1.5 %shard_map.159 = (bf16[32,512]{1,0:T(8,128)(2,1)}, f32[1,24,128,128]{3,2,1,0:T(8,128)}) custom-call(bf16[8,16,768]{2,1,0:T(8,128)(2,1)S(1)} %get-tuple-element.5.mg, f32[1,24,128,128]{3,2,1,0:T(8,128)S(1)} %get-tuple-element.6.carried, bf16[3072,512]{1,0:T(8,128)(2,1)S(1)} %get-tuple-element.7.w_out), custom_call_target="tpu_custom_call" | custom-call | tf_op jit(solution)/shard_map/pallas_call | solution.py:588
